TPU v7x, 32 devices: a whole 2x2x4 slice. The times are simulated.
32 devices in a mesh: sp: 16 (over z, y, x), tp: 2 (over core).
Axes of the slice: x: 2, y: 2, z: 4, core: 2. Of those that a mesh axis runs over, the one named last changes fastest.
Arguments:
- resid: bfloat16 [6144, 2048], P('sp'), may hold values from -6 to 6
- x_branch: bfloat16 [6144, 2048], P('sp', 'tp'), may hold values from -6 to 6
- gate_branch: bfloat16 [6144, 2048], P('sp', 'tp'), may hold values from -6 to 6
- conv_w: float32 [4, 2048], P(None, 'tp'), may hold values from -3 to 3
- gate_a_w: bfloat16 [32, 64, 64], P('tp'), may hold values from -0.75 to 0.75
- gate_x_w: bfloat16 [32, 64, 64], P('tp'), may hold values from -0.75 to 0.75
- decay_rate: float32 [2048], P('tp'), may hold values from 0 to 0.01, as said below
- decay_extra: float32 [6144, 2048], P('sp', 'tp'), may hold values from -3 to 0, as said below
- w_proj: bfloat16 [2048, 2048], P('tp'), may hold values from -0.125 to 0.125
- mix_gain: float32 [2048], replicated, may hold values from 0.1 to 1.9
- pre_gain: float32 [2048], replicated, may hold values from 0.1 to 1.9
- w_gate: bfloat16 [2048, 5632], P('sp', 'tp'), may hold values from -0.125 to 0.125
- w_up: bfloat16 [2048, 5632], P('sp', 'tp'), may hold values from -0.125 to 0.125
- w_down: bfloat16 [5632, 2048], P('tp', 'sp'), may hold values from -0.078125 to 0.078125
- out_gain: float32 [2048], replicated, may hold values from 0.1 to 1.9
Outputs:
- stream_out: bfloat16 [6144, 2048], P(('sp', 'tp'))
Inputs may be any that keep to these rules, and one draw needn't show every extreme that they name: `decay_rate`: positive rates. `decay_extra`: non-positive values.
All inputs are finite; a program needn't handle non-finite values.
Results may differ from a plain program's by a relative error of at most 0.015.
Values may be sent and summed in bfloat16 or wider, within the bound.
A program may use at most 128 MiB of HBM per device.

v0:
```python
import functools

import jax
import jax.numpy as jnp
from jax import lax
from jax.experimental import pallas as pl
from jax.experimental.pallas import tpu as pltpu
from jax.sharding import PartitionSpec as P

LRU_SCALE = 8.0
NORM_EPS = 1e-06
LANES = 128
SEGMENTS = 8
HALO = 16
MESH = pl.DeviceIdType.MESH


def neg_expm1(u):
    near = 1.0 + u * (1.0 / 8.0)
    for k in range(7, 1, -1):
        near = 1.0 + (u * (1.0 / k)) * near
    return jnp.where(u > -0.35, -u * near, 1.0 - jnp.exp(u))


def mixer_kernel(
    n,
    taps,
    x_ref,
    gate_ref,
    conv_ref,
    ga_ref,
    gx_ref,
    rate_ref,
    extra_ref,
    out_ref,
    halo,
    padded,
    decay,
    drive,
    seg_p,
    seg_h,
    mine,
    slots,
    halo_send,
    halo_recv,
    send_sems,
    recv_sems,
):
    me = lax.axis_index("sp")
    length, width = x_ref.shape
    blocks = width // LANES
    span = length // SEGMENTS

    barrier = pltpu.get_barrier_semaphore()

    def greet(k, carry):
        pl.semaphore_signal(
            barrier, inc=1, device_id={"sp": lax.rem(me + k, n)}, device_id_type=MESH
        )
        return carry

    lax.fori_loop(1, n, greet, 0)
    pl.semaphore_wait(barrier, n - 1)

    tail = pltpu.make_async_remote_copy(
        src_ref=x_ref.at[pl.ds(length - HALO, HALO)],
        dst_ref=halo,
        send_sem=halo_send,
        recv_sem=halo_recv,
        device_id={"sp": lax.rem(me + 1, n)},
        device_id_type=MESH,
    )
    tail.start()
    tail.wait()

    first_place = (me > 0).astype(jnp.float32)

    def one_block(c, carry):
        cols = pl.ds(pl.multiple_of(c * LANES, LANES), LANES)
        padded[pl.ds(8, length), :] = x_ref[:, cols].astype(jnp.float32)
        padded[pl.ds(0, 8), :] = halo[pl.ds(HALO - 8, 8), cols].astype(jnp.float32) * first_place
        start = 8 - (taps - 1)
        conv = padded[pl.ds(start, length), :] * conv_ref[pl.ds(0, 1), cols]
        for tap in range(1, taps):
            conv = conv + padded[pl.ds(start + tap, length), :] * conv_ref[pl.ds(tap, 1), cols]
        conv_out = conv.astype(jnp.bfloat16)
        recur = jax.nn.sigmoid(
            jnp.dot(conv_out, ga_ref[c], preferred_element_type=jnp.float32)
        )
        inject = jax.nn.sigmoid(
            jnp.dot(conv_out, gx_ref[c], preferred_element_type=jnp.float32)
        )
        log_decay = -LRU_SCALE * recur * rate_ref[pl.ds(0, 1), cols] + extra_ref[:, cols]
        decay[c] = jnp.exp(log_decay)
        room = neg_expm1(2.0 * log_decay)
        root = jnp.where(room > 0.0, jnp.sqrt(jnp.maximum(room, 1e-37)), 0.0)
        drive[c] = root * inject * conv_out.astype(jnp.float32)
        return carry

    lax.fori_loop(0, blocks, one_block, 0)

    def step(j, carry):
        prods, states = carry
        new_p, new_h = [], []
        for c in range(blocks):
            rows = pl.ds(j, SEGMENTS, stride=span)
            d = decay.at[c][rows, :]
            v = drive.at[c][rows, :]
            h = d * states[c] + v
            p = prods[c] * d
            drive.at[c][rows, :] = h
            decay.at[c][rows, :] = p
            new_h.append(h)
            new_p.append(p)
        return tuple(new_p), tuple(new_h)

    ones = tuple(jnp.ones((SEGMENTS, LANES), jnp.float32) for _ in range(blocks))
    zeros = tuple(jnp.zeros((SEGMENTS, LANES), jnp.float32) for _ in range(blocks))
    prods, states = lax.fori_loop(0, span, step, (ones, zeros))

    for c in range(blocks):
        p = jnp.ones((1, LANES), jnp.float32)
        h = jnp.zeros((1, LANES), jnp.float32)
        for s in range(SEGMENTS):
            seg_p[c, pl.ds(s, 1), :] = p
            seg_h[c, pl.ds(s, 1), :] = h
            h = prods[c][s : s + 1] * h + states[c][s : s + 1]
            p = p * prods[c][s : s + 1]
        mine[pl.ds(c, 1), :] = p
        mine[pl.ds(blocks + c, 1), :] = h

    def message(k):
        return pltpu.make_async_remote_copy(
            src_ref=mine,
            dst_ref=slots.at[k],
            send_sem=send_sems.at[k],
            recv_sem=recv_sems.at[k],
            device_id={"sp": lax.rem(me + k, n)},
            device_id_type=MESH,
        )

    def send(k, carry):
        message(k).start()
        return carry

    lax.fori_loop(1, n, send, 0)

    def one_gelu(c, carry):
        cols = pl.ds(pl.multiple_of(c * LANES, LANES), LANES)
        padded_gate = gate_ref[:, cols].astype(jnp.float32)
        out_f32 = jax.nn.gelu(padded_gate)
        seg = out_f32
        drive[c] = drive[c] * seg
        decay[c] = decay[c] * seg
        for s in range(SEGMENTS):
            rows = pl.ds(s * span, span)
            drive[c, rows, :] = drive[c, rows, :] + (
                decay[c, rows, :] * seg_h[c, pl.ds(s, 1), :]
            )
        return carry

    lax.fori_loop(0, blocks, one_gelu, 0)

    def receive(k, carry):
        message(k).wait()
        return carry

    lax.fori_loop(1, n, receive, 0)

    def compose(i, state):
        k = me - i
        part = slots[k]
        return part[:blocks] * state + part[blocks:]

    carried = lax.fori_loop(0, me, compose, jnp.zeros((blocks, LANES), jnp.float32))

    for c in range(blocks):
        for s in range(SEGMENTS):
            rows = pl.ds(s * span, span)
            entry = seg_p[c, pl.ds(s, 1), :] * carried[c : c + 1]
            out_ref[rows, pl.ds(c * LANES, LANES)] = (
                drive[c, rows, :] + decay[c, rows, :] * entry
            ).astype(jnp.bfloat16)


def diagonal(blocks):
    count, bw, _ = blocks.shape
    per = LANES // bw
    grouped = blocks.reshape(count // per, per, bw, bw)
    rows = []
    for i in range(per):
        rows.append(
            jnp.concatenate(
                [grouped[:, i] if i == j else jnp.zeros_like(grouped[:, i]) for j in range(per)],
                axis=-1,
            )
        )
    return jnp.concatenate(rows, axis=-2)


def mix(x_branch, gate_branch, conv_w, gate_a_w, gate_x_w, decay_rate, decay_extra):
    length, width = x_branch.shape
    n = lax.axis_size("sp")
    blocks = width // LANES
    vmem = pl.BlockSpec(memory_space=pltpu.VMEM)
    return pl.pallas_call(
        functools.partial(mixer_kernel, n, conv_w.shape[0]),
        out_shape=jax.ShapeDtypeStruct((length, width), jnp.bfloat16),
        in_specs=[vmem] * 7,
        out_specs=vmem,
        scratch_shapes=[
            pltpu.VMEM((HALO, width), jnp.bfloat16),
            pltpu.VMEM((length + 8, LANES), jnp.float32),
            pltpu.VMEM((blocks, length, LANES), jnp.float32),
            pltpu.VMEM((blocks, length, LANES), jnp.float32),
            pltpu.VMEM((blocks, SEGMENTS, LANES), jnp.float32),
            pltpu.VMEM((blocks, SEGMENTS, LANES), jnp.float32),
            pltpu.VMEM((2 * blocks, LANES), jnp.float32),
            pltpu.VMEM((n, 2 * blocks, LANES), jnp.float32),
            pltpu.SemaphoreType.DMA,
            pltpu.SemaphoreType.DMA,
            pltpu.SemaphoreType.DMA((n,)),
            pltpu.SemaphoreType.DMA((n,)),
        ],
        compiler_params=pltpu.CompilerParams(
            collective_id=0, has_side_effects=True, vmem_limit_bytes=24 * 1024 * 1024
        ),
        cost_estimate=pl.CostEstimate(
            flops=40_000 * length * width // 1024, bytes_accessed=12 * length * width, transcendentals=0
        ),
        name="mixer",
    )(
        x_branch,
        gate_branch,
        conv_w,
        diagonal(gate_a_w),
        diagonal(gate_x_w),
        decay_rate[None, :],
        decay_extra,
    )


VMEM = pl.BlockSpec(memory_space=pltpu.VMEM)


def lanes_at(block):
    return pl.ds(pl.multiple_of(block * LANES, LANES), LANES)


def pack_kernel(line, plane, gate_ref, up_ref, down_ref, *out_refs):
    part = gate_ref.shape[1] // line
    line_at = lax.axis_index("sp") // plane
    for z in range(line):
        units = pl.ds(z * part, part)
        flat = down_ref[units, :].astype(jnp.float32).T.astype(jnp.bfloat16)
        for s in range(line):

            @pl.when(lax.rem(line_at + s, line) == z)
            def _():
                out_refs[s][0, 0] = gate_ref[:, units]
                out_refs[s][1, 0] = up_ref[:, units]
                out_refs[s][2, 0] = flat


def pack(line, plane, w_gate, w_up, w_down):
    rows, units = w_gate.shape
    shape = jax.ShapeDtypeStruct((3, 1, rows, units // line), w_gate.dtype)
    return pl.pallas_call(
        functools.partial(pack_kernel, line, plane),
        out_shape=[shape] * line,
        in_specs=[VMEM] * 3,
        out_specs=[VMEM] * line,
        compiler_params=pltpu.CompilerParams(vmem_limit_bytes=24 * 1024 * 1024),
        name="pack",
    )(w_gate, w_up, w_down)


def ring_slot(ring, places, offset):
    plane = len(ring)
    here = lax.rem(lax.axis_index("sp"), plane)
    out = here * 0
    for p in range(plane):
        out = out + (here == p).astype(jnp.int32) * places(p, offset)
    return out


def enter_kernel(line, ring, count, *refs):
    parts, (resid_ref, mix_ref, pre_ref, stream_ref, mine_ref) = refs[:count], refs[count:]
    plane = len(ring)
    mixed = parts[0][...].astype(jnp.float32)
    for other in parts[1:]:
        mixed = mixed + other[...].astype(jnp.float32)
    stream = resid_ref[...].astype(jnp.float32) + rms_scale(mixed, mix_ref[...])
    stream_ref[...] = stream
    normed = rms_scale(stream, pre_ref[...]).astype(jnp.bfloat16)
    for p in range(plane):
        offset = ring_slot(ring, lambda q, p: (ring.index(p) - ring.index(q)) % plane, p)
        for z in range(line):
            at = (z * plane + p) * LANES
            mine_ref[:, lanes_at(offset * line + z)] = normed[:, at : at + LANES]


def enter(line, ring, parts, resid, mix_gain, pre_gain):
    share, width = resid.shape
    return pl.pallas_call(
        functools.partial(enter_kernel, line, ring, len(parts)),
        out_shape=[
            jax.ShapeDtypeStruct((share, width), jnp.float32),
            jax.ShapeDtypeStruct((share, width), jnp.bfloat16),
        ],
        in_specs=[VMEM] * (len(parts) + 3),
        out_specs=[VMEM] * 2,
        compiler_params=pltpu.CompilerParams(vmem_limit_bytes=24 * 1024 * 1024),
        name="enter",
    )(*parts, resid, mix_gain[None, :], pre_gain[None, :])


def leave_kernel(line, ring, own_ref, up_ref, down_ref, stream_ref, gain_ref, out_ref, ffn_ref):
    plane = len(ring)
    ffn = own_ref[...] + up_ref[...].astype(jnp.float32) + down_ref[...].astype(jnp.float32)
    ffn_ref[...] = ffn * (
        0.5 * lax.rsqrt(jnp.mean(ffn * ffn, axis=-1, keepdims=True) + NORM_EPS)
    )
    for p in range(plane):
        offset = ring_slot(ring, lambda q, p: (ring.index(p) - ring.index(q)) % plane, p)
        for z in range(line):
            cols = pl.ds((z * plane + p) * LANES, LANES)
            out_ref[:, cols] = (
                stream_ref[:, cols] + ffn_ref[:, lanes_at(offset * line + z)] * gain_ref[:, cols]
            ).astype(jnp.bfloat16)


def leave(line, ring, own, up_sum, down_sum, stream, out_gain):
    share, width = stream.shape
    return pl.pallas_call(
        functools.partial(leave_kernel, line, ring),
        out_shape=jax.ShapeDtypeStruct((share, width), jnp.bfloat16),
        in_specs=[VMEM] * 5,
        out_specs=VMEM,
        scratch_shapes=[pltpu.VMEM((share, width), jnp.float32)],
        compiler_params=pltpu.CompilerParams(vmem_limit_bytes=24 * 1024 * 1024),
        name="leave",
    )(own, up_sum, down_sum, stream, out_gain[None, :])


def hidden_kernel(tokens_ref, *refs):
    weights, out_ref = refs[:-1], refs[-1]
    gate = upward = None
    at = 0
    for w in weights:
        block = tokens_ref[:, at : at + w.shape[1]]
        g = jnp.dot(block, w[0], preferred_element_type=jnp.float32)
        u = jnp.dot(block, w[1], preferred_element_type=jnp.float32)
        gate = g if gate is None else gate + g
        upward = u if upward is None else upward + u
        at += w.shape[1]
    hidden = (jax.nn.silu(gate) * upward).astype(jnp.bfloat16)
    at = 0
    for w in weights:
        out_ref[:, at : at + w.shape[1]] = lax.dot_general(
            hidden, w[2], (((1,), (1,)), ((), ())), preferred_element_type=jnp.float32
        ).astype(jnp.bfloat16)
        at += w.shape[1]


def feed(tokens, pieces):
    rows, width = tokens.shape
    block = rows // 2
    part = pieces[0].shape[2]
    return pl.pallas_call(
        hidden_kernel,
        grid=(rows // block,),
        out_shape=jax.ShapeDtypeStruct((rows, width), jnp.bfloat16),
        in_specs=[pl.BlockSpec((block, width), lambda i: (i, 0))]
        + [pl.BlockSpec(p.shape, lambda i: (0, 0, 0)) for p in pieces],
        out_specs=pl.BlockSpec((block, width), lambda i: (i, 0)),
        compiler_params=pltpu.CompilerParams(vmem_limit_bytes=48 * 1024 * 1024),
        cost_estimate=pl.CostEstimate(
            flops=6 * rows * width * part, bytes_accessed=6 * width * part, transcendentals=0
        ),
        name="feed",
    )(tokens, *pieces)


def rms_scale(values, gains):
    return values * lax.rsqrt(jnp.mean(values * values, axis=-1, keepdims=True) + NORM_EPS) * gains


def shift(value, axis, steps):
    count = lax.axis_size(axis)
    return lax.ppermute(value, axis, [(i, (i + steps) % count) for i in range(count)])


def shards(
    resid,
    x_branch,
    gate_branch,
    conv_w,
    gate_a_w,
    gate_x_w,
    decay_rate,
    decay_extra,
    w_proj,
    mix_gain,
    pre_gain,
    w_gate,
    w_up,
    w_down,
    out_gain,
):
    n = lax.axis_size("sp")
    tp = lax.axis_size("tp")
    sp_at = lax.axis_index("sp")
    tp_at = lax.axis_index("tp")
    line = 4
    plane = n // line
    line_at = sp_at // plane
    plane_at = sp_at % plane
    ring = [0, 1, 3, 2] if plane == 4 else list(range(plane))
    ring_of = [ring.index(p) for p in range(plane)]

    def along_line(value, steps):
        pairs = [
            (z * plane + p, (z + steps) * plane + p)
            for z in range(line)
            for p in range(plane)
            if 0 <= z + steps < line
        ]
        return lax.ppermute(value, "sp", pairs)

    def round_line(value, steps):
        pairs = [
            (z * plane + p, ((z + steps) % line) * plane + p)
            for z in range(line)
            for p in range(plane)
        ]
        return lax.ppermute(value, "sp", pairs)

    def round_plane(value, steps):
        pairs = [
            (z * plane + ring[i], z * plane + ring[(i + steps) % plane])
            for z in range(line)
            for i in range(plane)
        ]
        return lax.ppermute(value, "sp", pairs)

    rows, units = w_gate.shape
    part = units // line
    aligned = rows % LANES == 0 and plane == 4
    if aligned:
        bundles = pack(line, plane, w_gate, w_up, w_down)
    else:
        packed = jnp.stack(
            [
                jnp.stack([w[:, z * part : (z + 1) * part] for z in range(line)])
                for w in (w_gate, w_up)
            ]
            + [w_down.reshape(line, part, rows).transpose(0, 2, 1)],
            axis=1,
        )
        bundles = [
            lax.dynamic_index_in_dim(packed, (line_at + s) % line, 0, True).transpose(1, 0, 2, 3)
            for s in range(line)
        ]
    stack = jnp.zeros((3, line, rows, part), w_gate.dtype)
    stack = lax.dynamic_update_slice_in_dim(stack, bundles[0], line_at, 1)
    arrived = []
    for s in range(1, line):
        arrived.append((s, round_line(bundles[s], s)))
    for s, piece in arrived:
        stack = lax.dynamic_update_slice_in_dim(stack, piece, (line_at - s) % line, 1)
    from_ring = {0: [stack]}
    ahead = behind = stack
    for k in range(1, plane // 2):
        ahead = round_plane(ahead, -1)
        behind = round_plane(behind, 1)
        from_ring[k] = [ahead]
        from_ring[plane - k] = [behind]
    low = round_plane(ahead[:, : line // 2], -1)
    high = round_plane(behind[:, line // 2 :], 1)
    from_ring[plane // 2] = [low, high]
    ring_at = jnp.asarray(ring_of)[plane_at]

    order = jnp.asarray(ring)[(ring_at + jnp.arange(plane)) % plane]
    back = (jnp.asarray(ring_of) - ring_at) % plane

    mixer = mix(x_branch, gate_branch, conv_w, gate_a_w, gate_x_w, decay_rate, decay_extra)
    length = mixer.shape[0]
    share = length // tp
    width = w_proj.shape[1]
    partial = jnp.dot(mixer, w_proj, preferred_element_type=jnp.float32).astype(jnp.bfloat16)

    def share_of(value, place):
        return lax.dynamic_slice_in_dim(value, place * share, share, 0)

    parts = [share_of(partial, tp_at)]
    for i in range(1, tp):
        parts.append(shift(share_of(partial, (tp_at + i) % tp), "tp", i))
    own_resid = share_of(resid, tp_at)
    if aligned:
        stream, mine = enter(line, ring, parts, own_resid, mix_gain, pre_gain)
    else:
        mixed = sum(part.astype(jnp.float32) for part in parts)
        stream = own_resid.astype(jnp.float32) + rms_scale(mixed, mix_gain)
        normed = rms_scale(stream, pre_gain).astype(jnp.bfloat16)
        cut = normed.reshape(share, line, plane, rows)
        mine = jnp.stack(
            [lax.dynamic_index_in_dim(cut, order[j], 2, False) for j in range(plane)], axis=1
        ).reshape(share, width)

    up = down = mine
    ups, downs = [], []
    for _ in range(1, line):
        up = along_line(up, 1)
        down = along_line(down, -1)
        ups.append(up)
        downs.append(down)
    slots = [mine]
    for k in range(1, line):
        slots.append(jnp.where(line_at >= k, ups[k - 1], downs[line - k - 1]))

    pieces = []
    for j in range(plane):
        for piece in from_ring[j]:
            pieces.append(piece.reshape(3, piece.shape[1] * rows, part))

    def feed_forward(chosen):
        own_rows = jnp.concatenate([slots[k] for k in chosen], axis=0)
        tokens = [own_rows] + [shift(own_rows, "tp", -i) for i in range(1, tp)]
        out = feed(jnp.concatenate(tokens, axis=0), pieces)
        out = out.reshape(tp, len(chosen) * share, width)
        total = out[0].astype(jnp.float32)
        for i in range(1, tp):
            total = total + shift(out[i], "tp", i).astype(jnp.float32)
        return {k: total[a * share : (a + 1) * share] for a, k in enumerate(chosen)}

    sums = {}
    for chosen in ([2, 0], [1, 3]) if line == 4 else ([k for k in range(line)],):
        sums.update(feed_forward(chosen))

    up_sum = down_sum = None
    for k in range(line - 1, 0, -1):
        to_up, to_down = sums[line - k], sums[k]
        if up_sum is not None:
            to_up = to_up + up_sum.astype(jnp.float32)
            to_down = to_down + down_sum.astype(jnp.float32)
        up_sum = along_line(to_up.astype(jnp.bfloat16), 1)
        down_sum = along_line(to_down.astype(jnp.bfloat16), -1)
    if aligned:
        return leave(line, ring, sums[0], up_sum, down_sum, stream, out_gain)
    ffn = sums[0] + up_sum.astype(jnp.float32) + down_sum.astype(jnp.float32)
    ffn = ffn.reshape(share, plane, line, rows)
    ffn = jnp.stack(
        [lax.dynamic_index_in_dim(ffn, back[p], 1, False) for p in range(plane)], axis=2
    ).reshape(share, width)
    return (stream + 0.5 * rms_scale(ffn, out_gain)).astype(jnp.bfloat16)


def solution(mesh):
    return jax.shard_map(
        shards,
        mesh=mesh,
        in_specs=(
            P("sp", None),
            P("sp", "tp"),
            P("sp", "tp"),
            P(None, "tp"),
            P("tp", None, None),
            P("tp", None, None),
            P("tp"),
            P("sp", "tp"),
            P("tp", None),
            P(),
            P(),
            P("sp", "tp"),
            P("sp", "tp"),
            P("tp", "sp"),
            P(),
        ),
        out_specs=P(("sp", "tp"), None),
        check_vma=False,
    )
```

profile of v0, /device:TPU:0, one launch (start us, length us, event | category | flops | bytes accessed | tf_op | source)
XLA Modules:
  0.0 307.5 jit_solution(13109142053959926223)
XLA Ops:
  6.9 20.2 %mixer.1 = bf16[384,1024]{1,0:T(8,128)(2,1)S(1)} custom-call(bf16[384,1024]{1,0:T(8,128)(2,1)S(1)} %copy-done.7, bf16[384,1024]{1,0:T(8,128)(2,1)S(1)} %copy-done.8, f32[4,1024]{1,0:T(4,128)S(1)} %copy-done.12, bf16[8,128,128]{2,1,0:T(8,128)(2,1)S(1)} %get-tuple-element.30.ga_ref, bf16[8,128,128]{2,1,0:T(8,128)(2,1)S(1)} %get-tuple-element.31.gx_ref, ...), custom_call_target="tpu_custom_call" | custom-call | flops 15360000 | bytes 4718592 | tf_op jit(solution)/shard_map/mixer/pallas_call | solution.py:206
  34.9 5.4 %collective-permute-start.1 = (bf16[192,2048]{1,0:T(8,128)(2,1)S(1)}, bf16[192,2048]{1,0:T(8,128)(2,1)}, u32[]{:S(2)}, u32[]{:S(2)}) collective-permute-start(bf16[192,2048]{1,0:T(8,128)(2,1)S(1)} %get-tuple-element.11), channel_id=1, source_target_pairs={{0,8},{2,10},{4,12},{6,14},{8,16},{10,18},{12,20},{14,22},{16,24},... | collective-permute-start | bytes 2359304 | tf_op jit(solution)/shard_map/ppermute | solution.py:429
  40.4 14.8 %collective-permute-done.3 = bf16[192,2048]{1,0:T(8,128)(2,1)} collective-permute-done((bf16[192,2048]{1,0:T(8,128)(2,1)S(1)}, bf16[192,2048]{1,0:T(8,128)(2,1)}, u32[]{:S(2)}, u32[]{:S(2)}) %collective-permute-start.3) | collective-permute-done | bytes 786464 | tf_op jit(solution)/shard_map/ppermute | solution.py:429
  62.3 2.9 collective-permute-start.7
  65.2 2.8 collective-permute-start.2
  69.4 21.2 %collective-permute-done.4 = bf16[192,2048]{1,0:T(8,128)(2,1)} collective-permute-done((bf16[192,2048]{1,0:T(8,128)(2,1)}, bf16[192,2048]{1,0:T(8,128)(2,1)}, u32[]{:S(2)}, u32[]{:S(2)}) %collective-permute-start.4) | collective-permute-done | bytes 786464 | tf_op jit(solution)/shard_map/ppermute | solution.py:429
  93.6 19.5 %collective-permute-done.7 = bf16[3,1,128,704]{2,3,1,0:T(8,128)(2,1)} collective-permute-done((bf16[3,1,128,704]{2,3,1,0:T(8,128)(2,1)}, bf16[3,1,128,704]{2,3,1,0:T(8,128)(2,1)}, u32[]{:S(2)}, u32[]{:S(2)}) %collective-permute-start.7) | collective-permute-done | bytes 540704 | tf_op jit(solution)/shard_map/ppermute | solution.py:437
  117.4 13.9 %collective-permute-start.15 = (bf16[192,2048]{1,0:T(8,128)(2,1)}, bf16[192,2048]{1,0:T(8,128)(2,1)}, u32[]{:S(2)}, u32[]{:S(2)}) collective-permute-start(bf16[192,2048]{1,0:T(8,128)(2,1)} %collective-permute-done.2), channel_id=1, source_target_pairs={{0,8},{2,10},{4,12},{6,14},{8,16},{10,18},{12,20},{14,22},{16,24},... | collective-permute-start | bytes 2359304 | tf_op jit(solution)/shard_map/ppermute | solution.py:429
  132.5 11.2 %collective-permute-done.15 = bf16[192,2048]{1,0:T(8,128)(2,1)} collective-permute-done((bf16[192,2048]{1,0:T(8,128)(2,1)}, bf16[192,2048]{1,0:T(8,128)(2,1)}, u32[]{:S(2)}, u32[]{:S(2)}) %collective-permute-start.15) | collective-permute-done | bytes 786464 | tf_op jit(solution)/shard_map/ppermute | solution.py:429
  146.4 14.8 %collective-permute-done.11 = bf16[3,4,128,704]{2,3,1,0:T(8,128)(2,1)} collective-permute-done((bf16[3,4,128,704]{2,3,1,0:T(8,128)(2,1)S(1)}, bf16[3,4,128,704]{2,3,1,0:T(8,128)(2,1)}, u32[]{:S(2)}, u32[]{:S(2)}) %collective-permute-start.11) | collective-permute-done | bytes 2162720 | tf_op jit(solution)/shard_map/ppermute | solution.py:445
  170.4 2.8 copy.28
  173.2 4.3 %copy.32 = bf16[3,4,128,704]{3,2,1,0:T(8,128)(2,1)} copy(bf16[3,4,128,704]{2,3,1,0:T(8,128)(2,1)} %collective-permute-done.11) | data formatting | bytes 4325376 | tf_op jit(solution)/shard_map/ppermute | solution.py:445
  177.5 4.2 %copy.29 = bf16[3,4,128,704]{3,2,1,0:T(8,128)(2,1)} copy(bf16[3,4,128,704]{2,3,1,0:T(8,128)(2,1)} %collective-permute-done.9) | data formatting | bytes 4325376 | tf_op jit(solution)/shard_map/ppermute | solution.py:445
  181.7 3.7 %collective-permute-done.12 = bf16[3,2,128,704]{2,3,1,0:T(8,128)(2,1)} collective-permute-done((bf16[3,2,128,704]{2,3,1,0:T(8,128)(2,1)}, bf16[3,2,128,704]{2,3,1,0:T(8,128)(2,1)}, u32[]{:S(2)}, u32[]{:S(2)}) %collective-permute-start.12) | collective-permute-done | bytes 1081376 | tf_op jit(solution)/shard_map/ppermute | solution.py:445
  191.4 4.1 %pad_maximum_fusion.1.tokens_ref = bf16[768,2048]{1,0:T(8,128)(2,1)} fusion(bf16[384,2048]{1,0:T(8,128)(2,1)} %collective-permute-done.16, bf16[192,2048]{1,0:T(8,128)(2,1)} %copy-done.19, bf16[192,2048]{1,0:T(8,128)(2,1)} %copy-done.18), kind=kLoop, calls=%fused_computation.1 | loop fusion | flops 9437184 | bytes 6291456 | tf_op jit(solution)/shard_map/concatenate | solution.py:530
  195.5 11.7 %feed.3 = bf16[768,2048]{1,0:T(8,128)(2,1)} custom-call(bf16[768,2048]{1,0:T(8,128)(2,1)} %pad_maximum_fusion.1.tokens_ref, bf16[3,512,704]{2,1,0:T(8,128)(2,1)S(1)} %bitcast.29, bf16[3,512,704]{2,1,0:T(8,128)(2,1)} %bitcast.41, bf16[3,256,704]{2,1,0:T(8,128)(2,1)S(1)} %bitcast.33, bf16[3,256,704]{2,1,0:T(8,128)(2,1)S(1)} %bitcast.31, ...), custom_call_target="tpu_custom_call" | custom-call | flops 6643777536 | bytes 8650752 | tf_op jit(solution)/shard_map/feed/pallas_call | solution.py:370
  208.9 3.4 %pad_maximum_fusion.tokens_ref = bf16[768,2048]{1,0:T(8,128)(2,1)} fusion(bf16[384,2048]{1,0:T(8,128)(2,1)} %collective-permute-done.5, bf16[192,2048]{1,0:T(8,128)(2,1)S(1)} %get-tuple-element.11, bf16[192,2048]{1,0:T(8,128)(2,1)S(1)} %copy-done.21), kind=kLoop, calls=%fused_computation | loop fusion | flops 9437184 | bytes 6291456 | tf_op jit(solution)/shard_map/concatenate | solution.py:530
  212.4 11.7 %feed.2 = bf16[768,2048]{1,0:T(8,128)(2,1)} custom-call(bf16[768,2048]{1,0:T(8,128)(2,1)} %pad_maximum_fusion.tokens_ref, bf16[3,512,704]{2,1,0:T(8,128)(2,1)S(1)} %bitcast.30, bf16[3,512,704]{2,1,0:T(8,128)(2,1)} %bitcast.42, bf16[3,256,704]{2,1,0:T(8,128)(2,1)S(1)} %bitcast.34, bf16[3,256,704]{2,1,0:T(8,128)(2,1)S(1)} %bitcast.32, ...), custom_call_target="tpu_custom_call" | custom-call | flops 6643777536 | bytes 8650752 | tf_op jit(solution)/shard_map/feed/pallas_call | solution.py:370
  228.7 13.6 %collective-permute-start.18 = (bf16[192,2048]{1,0:T(8,128)(2,1)S(1)}, bf16[192,2048]{1,0:T(8,128)(2,1)S(1)}, u32[]{:S(2)}, u32[]{:S(2)}) collective-permute-start(bf16[192,2048]{1,0:T(8,128)(2,1)S(1)} %get-tuple-element.23), channel_id=1, source_target_pairs={{0,8},{2,10},{4,12},{6,14},{8,16},{10,18},{12,20},{14,22},{16,24},... | collective-permute-start | bytes 2359304 | tf_op jit(solution)/shard_map/ppermute | solution.py:429
  242.9 15.6 %collective-permute-done.21 = bf16[192,2048]{1,0:T(8,128)(2,1)S(1)} collective-permute-done((bf16[192,2048]{1,0:T(8,128)(2,1)S(1)}, bf16[192,2048]{1,0:T(8,128)(2,1)S(1)}, u32[]{:S(2)}, u32[]{:S(2)}) %collective-permute-start.21) | collective-permute-done | bytes 786464 | tf_op jit(solution)/shard_map/ppermute | solution.py:429
  261.5 5.2 %collective-permute-start.19 = (bf16[192,2048]{1,0:T(8,128)(2,1)S(1)}, bf16[192,2048]{1,0:T(8,128)(2,1)S(1)}, u32[]{:S(2)}, u32[]{:S(2)}) collective-permute-start(bf16[192,2048]{1,0:T(8,128)(2,1)S(1)} %get-tuple-element.20), channel_id=1, source_target_pairs={{0,8},{2,10},{4,12},{6,14},{8,16},{10,18},{12,20},{14,22},{16,24},... | collective-permute-start | bytes 2359304 | tf_op jit(solution)/shard_map/ppermute | solution.py:429
  266.7 15.2 %collective-permute-done.22 = bf16[192,2048]{1,0:T(8,128)(2,1)S(1)} collective-permute-done((bf16[192,2048]{1,0:T(8,128)(2,1)S(1)}, bf16[192,2048]{1,0:T(8,128)(2,1)S(1)}, u32[]{:S(2)}, u32[]{:S(2)}) %collective-permute-start.22) | collective-permute-done | bytes 786464 | tf_op jit(solution)/shard_map/ppermute | solution.py:429
  285.1 5.1 %collective-permute-start.20 = (bf16[192,2048]{1,0:T(8,128)(2,1)S(1)}, bf16[192,2048]{1,0:T(8,128)(2,1)S(1)}, u32[]{:S(2)}, u32[]{:S(2)}) collective-permute-start(bf16[192,2048]{1,0:T(8,128)(2,1)S(1)} %get-tuple-element.18), channel_id=1, source_target_pairs={{0,8},{2,10},{4,12},{6,14},{8,16},{10,18},{12,20},{14,22},{16,24},... | collective-permute-start | bytes 2359304 | tf_op jit(solution)/shard_map/ppermute | solution.py:429
  290.1 14.5 %collective-permute-done.23.down_ref = bf16[192,2048]{1,0:T(8,128)(2,1)S(1)} collective-permute-done((bf16[192,2048]{1,0:T(8,128)(2,1)S(1)}, bf16[192,2048]{1,0:T(8,128)(2,1)S(1)}, u32[]{:S(2)}, u32[]{:S(2)}) %collective-permute-start.23) | collective-permute-done | bytes 786464 | tf_op jit(solution)/shard_map/ppermute | solution.py:429
  (116 shorter events, 65.0 us)
Async XLA Ops:
  29.0 2.4 collective-permute-start
  33.6 21.6 %collective-permute-start.3 = (bf16[192,2048]{1,0:T(8,128)(2,1)S(1)}, bf16[192,2048]{1,0:T(8,128)(2,1)}, u32[]{:S(2)}, u32[]{:S(2)}) collective-permute-start(bf16[192,2048]{1,0:T(8,128)(2,1)S(1)} %get-tuple-element.11), channel_id=1, source_target_pairs={{8,0},{10,2},{12,4},{14,6},{16,8},{18,10},{20,12},{22,14},{24,16},... | collective-permute-start | bytes 2359304 | tf_op jit(solution)/shard_map/ppermute | solution.py:429
  34.9 30.3 %collective-permute-start.1 = (bf16[192,2048]{1,0:T(8,128)(2,1)S(1)}, bf16[192,2048]{1,0:T(8,128)(2,1)}, u32[]{:S(2)}, u32[]{:S(2)}) collective-permute-start(bf16[192,2048]{1,0:T(8,128)(2,1)S(1)} %get-tuple-element.11), channel_id=1, source_target_pairs={{0,8},{2,10},{4,12},{6,14},{8,16},{10,18},{12,20},{14,22},{16,24},... | collective-permute-start | bytes 2359304 | tf_op jit(solution)/shard_map/ppermute | solution.py:429
  55.2 35.4 %collective-permute-start.4 = (bf16[192,2048]{1,0:T(8,128)(2,1)}, bf16[192,2048]{1,0:T(8,128)(2,1)}, u32[]{:S(2)}, u32[]{:S(2)}) collective-permute-start(bf16[192,2048]{1,0:T(8,128)(2,1)} %collective-permute-done.3), channel_id=1, source_target_pairs={{8,0},{10,2},{12,4},{14,6},{16,8},{18,10},{20,12},{22,14},{24,16},... | collective-permute-start | bytes 2359304 | tf_op jit(solution)/shard_map/ppermute | solution.py:429
  58.6 33.9 %collective-permute-start.6 = (bf16[3,1,128,704]{2,3,1,0:T(8,128)(2,1)}, bf16[3,1,128,704]{2,3,1,0:T(8,128)(2,1)}, u32[]{:S(2)}, u32[]{:S(2)}) collective-permute-start(bf16[3,1,128,704]{2,3,1,0:T(8,128)(2,1)} %copy.25), channel_id=1, source_target_pairs={{0,8},{2,10},{4,12},{6,14},{8,16},{10,18},{12,20},{14,22},{16,24},... | collective-permute-start | bytes 1622024 | tf_op jit(solution)/shard_map/ppermute | solution.py:437
  62.3 50.8 %collective-permute-start.7 = (bf16[3,1,128,704]{2,3,1,0:T(8,128)(2,1)}, bf16[3,1,128,704]{2,3,1,0:T(8,128)(2,1)}, u32[]{:S(2)}, u32[]{:S(2)}) collective-permute-start(bf16[3,1,128,704]{2,3,1,0:T(8,128)(2,1)} %copy.26), channel_id=1, source_target_pairs={{0,16},{2,18},{4,20},{6,22},{8,24},{10,26},{12,28},{14,30},{16,0},... | collective-permute-start | bytes 1622024 | tf_op jit(solution)/shard_map/ppermute | solution.py:437
  65.2 52.2 %collective-permute-start.2 = (bf16[192,2048]{1,0:T(8,128)(2,1)}, bf16[192,2048]{1,0:T(8,128)(2,1)}, u32[]{:S(2)}, u32[]{:S(2)}) collective-permute-start(bf16[192,2048]{1,0:T(8,128)(2,1)} %collective-permute-done.1), channel_id=1, source_target_pairs={{0,8},{2,10},{4,12},{6,14},{8,16},{10,18},{12,20},{14,22},{16,24},... | collective-permute-start | bytes 2359304 | tf_op jit(solution)/shard_map/ppermute | solution.py:429
  69.1 45.1 %collective-permute-start.8 = (bf16[3,1,128,704]{2,3,1,0:T(8,128)(2,1)}, bf16[3,1,128,704]{2,3,1,0:T(8,128)(2,1)}, u32[]{:S(2)}, u32[]{:S(2)}) collective-permute-start(bf16[3,1,128,704]{2,3,1,0:T(8,128)(2,1)} %copy.27), channel_id=1, source_target_pairs={{0,24},{2,26},{4,28},{6,30},{8,0},{10,2},{12,4},{14,6},{16,8},{18,... | collective-permute-start | bytes 1622024 | tf_op jit(solution)/shard_map/ppermute | solution.py:437
  90.7 40.6 %collective-permute-start.14 = (bf16[192,2048]{1,0:T(8,128)(2,1)}, bf16[192,2048]{1,0:T(8,128)(2,1)}, u32[]{:S(2)}, u32[]{:S(2)}) collective-permute-start(bf16[192,2048]{1,0:T(8,128)(2,1)} %collective-permute-done.4), channel_id=1, source_target_pairs={{8,0},{10,2},{12,4},{14,6},{16,8},{18,10},{20,12},{22,14},{24,16},... | collective-permute-start | bytes 2359304 | tf_op jit(solution)/shard_map/ppermute | solution.py:429
  115.3 45.8 %collective-permute-start.11 = (bf16[3,4,128,704]{2,3,1,0:T(8,128)(2,1)S(1)}, bf16[3,4,128,704]{2,3,1,0:T(8,128)(2,1)}, u32[]{:S(2)}, u32[]{:S(2)}) collective-permute-start(bf16[3,4,128,704]{2,3,1,0:T(8,128)(2,1)S(1)} %constant_dynamic-update-slice_fusion), channel_id=1, source_target_pairs={{0,2},{2,6},{6,4},{4,0},{8,10},{10,14},{14,12},{12,8},{16,18},{18,... | collective-permute-start | bytes 6488072 | tf_op jit(solution)/shard_map/ppermute | solution.py:445
  116.9 48.1 %collective-permute-start.9 = (bf16[3,4,128,704]{2,3,1,0:T(8,128)(2,1)S(1)}, bf16[3,4,128,704]{2,3,1,0:T(8,128)(2,1)}, u32[]{:S(2)}, u32[]{:S(2)}) collective-permute-start(bf16[3,4,128,704]{2,3,1,0:T(8,128)(2,1)S(1)} %constant_dynamic-update-slice_fusion), channel_id=1, source_target_pairs={{0,4},{2,0},{6,2},{4,6},{8,12},{10,8},{14,10},{12,14},{16,20},{18,... | collective-permute-start | bytes 6488072 | tf_op jit(solution)/shard_map/ppermute | solution.py:445
  117.4 26.4 %collective-permute-start.15 = (bf16[192,2048]{1,0:T(8,128)(2,1)}, bf16[192,2048]{1,0:T(8,128)(2,1)}, u32[]{:S(2)}, u32[]{:S(2)}) collective-permute-start(bf16[192,2048]{1,0:T(8,128)(2,1)} %collective-permute-done.2), channel_id=1, source_target_pairs={{0,8},{2,10},{4,12},{6,14},{8,16},{10,18},{12,20},{14,22},{16,24},... | collective-permute-start | bytes 2359304 | tf_op jit(solution)/shard_map/ppermute | solution.py:429
  146.4 45.0 %collective-permute-start.16 = (bf16[384,2048]{1,0:T(8,128)(2,1)}, bf16[384,2048]{1,0:T(8,128)(2,1)}, u32[]{:S(2)}, u32[]{:S(2)}) collective-permute-start(bf16[384,2048]{1,0:T(8,128)(2,1)} %pad_maximum_fusion.3), channel_id=1, source_target_pairs={{0,1},{1,0},{2,3},{3,2},{4,5},{5,4},{6,7},{7,6},{8,9},{9,8},{10,11... | collective-permute-start | bytes 4718600 | tf_op jit(solution)/shard_map/ppermute | solution.py:391
  163.5 22.0 %collective-permute-start.12 = (bf16[3,2,128,704]{2,3,1,0:T(8,128)(2,1)}, bf16[3,2,128,704]{2,3,1,0:T(8,128)(2,1)}, u32[]{:S(2)}, u32[]{:S(2)}) collective-permute-start(bf16[3,2,128,704]{2,3,1,0:T(8,128)(2,1)} %slice.65), channel_id=1, source_target_pairs={{0,2},{2,6},{6,4},{4,0},{8,10},{10,14},{14,12},{12,8},{16,18},{18,... | collective-permute-start | bytes 3244040 | tf_op jit(solution)/shard_map/ppermute | solution.py:445
  167.3 21.7 %collective-permute-start.10 = (bf16[3,2,128,704]{2,3,1,0:T(8,128)(2,1)}, bf16[3,2,128,704]{2,3,1,0:T(8,128)(2,1)}, u32[]{:S(2)}, u32[]{:S(2)}) collective-permute-start(bf16[3,2,128,704]{2,3,1,0:T(8,128)(2,1)} %slice.64), channel_id=1, source_target_pairs={{0,4},{2,0},{6,2},{4,6},{8,12},{10,8},{14,10},{12,14},{16,20},{18,... | collective-permute-start | bytes 3244040 | tf_op jit(solution)/shard_map/ppermute | solution.py:445
  170.4 38.5 %collective-permute-start.5 = (bf16[384,2048]{1,0:T(8,128)(2,1)}, bf16[384,2048]{1,0:T(8,128)(2,1)}, u32[]{:S(2)}, u32[]{:S(2)}) collective-permute-start(bf16[384,2048]{1,0:T(8,128)(2,1)} %pad_maximum_fusion.2), channel_id=1, source_target_pairs={{0,1},{1,0},{2,3},{3,2},{4,5},{5,4},{6,7},{7,6},{8,9},{9,8},{10,11... | collective-permute-start | bytes 4718600 | tf_op jit(solution)/shard_map/ppermute | solution.py:391
  208.8 17.5 %collective-permute-start.17 = (bf16[384,2048]{1,0:T(8,128)(2,1)S(1)}, bf16[384,2048]{1,0:T(8,128)(2,1)S(1)}, u32[]{:S(2)}, u32[]{:S(2)}) collective-permute-start(bf16[384,2048]{1,0:T(8,128)(2,1)S(1)} %slice.70), channel_id=1, source_target_pairs={{0,1},{1,0},{2,3},{3,2},{4,5},{5,4},{6,7},{7,6},{8,9},{9,8},{10,11... | collective-permute-start | bytes 4718600 | tf_op jit(solution)/shard_map/ppermute | solution.py:391
  225.8 16.5 %collective-permute-start.13 = (bf16[384,2048]{1,0:T(8,128)(2,1)S(1)}, bf16[384,2048]{1,0:T(8,128)(2,1)S(1)}, u32[]{:S(2)}, u32[]{:S(2)}) collective-permute-start(bf16[384,2048]{1,0:T(8,128)(2,1)S(1)} %slice.67), channel_id=1, source_target_pairs={{0,1},{1,0},{2,3},{3,2},{4,5},{5,4},{6,7},{7,6},{8,9},{9,8},{10,11... | collective-permute-start | bytes 4718600 | tf_op jit(solution)/shard_map/ppermute | solution.py:391
  227.3 31.2 %collective-permute-start.21 = (bf16[192,2048]{1,0:T(8,128)(2,1)S(1)}, bf16[192,2048]{1,0:T(8,128)(2,1)S(1)}, u32[]{:S(2)}, u32[]{:S(2)}) collective-permute-start(bf16[192,2048]{1,0:T(8,128)(2,1)S(1)} %get-tuple-element.22), channel_id=1, source_target_pairs={{8,0},{10,2},{12,4},{14,6},{16,8},{18,10},{20,12},{22,14},{24,16},... | collective-permute-start | bytes 2359304 | tf_op jit(solution)/shard_map/ppermute | solution.py:429
  228.7 31.0 %collective-permute-start.18 = (bf16[192,2048]{1,0:T(8,128)(2,1)S(1)}, bf16[192,2048]{1,0:T(8,128)(2,1)S(1)}, u32[]{:S(2)}, u32[]{:S(2)}) collective-permute-start(bf16[192,2048]{1,0:T(8,128)(2,1)S(1)} %get-tuple-element.23), channel_id=1, source_target_pairs={{0,8},{2,10},{4,12},{6,14},{8,16},{10,18},{12,20},{14,22},{16,24},... | collective-permute-start | bytes 2359304 | tf_op jit(solution)/shard_map/ppermute | solution.py:429
  260.2 21.7 %collective-permute-start.22 = (bf16[192,2048]{1,0:T(8,128)(2,1)S(1)}, bf16[192,2048]{1,0:T(8,128)(2,1)S(1)}, u32[]{:S(2)}, u32[]{:S(2)}) collective-permute-start(bf16[192,2048]{1,0:T(8,128)(2,1)S(1)} %get-tuple-element.19), channel_id=1, source_target_pairs={{8,0},{10,2},{12,4},{14,6},{16,8},{18,10},{20,12},{22,14},{24,16},... | collective-permute-start | bytes 2359304 | tf_op jit(solution)/shard_map/ppermute | solution.py:429
  261.5 21.7 %collective-permute-start.19 = (bf16[192,2048]{1,0:T(8,128)(2,1)S(1)}, bf16[192,2048]{1,0:T(8,128)(2,1)S(1)}, u32[]{:S(2)}, u32[]{:S(2)}) collective-permute-start(bf16[192,2048]{1,0:T(8,128)(2,1)S(1)} %get-tuple-element.20), channel_id=1, source_target_pairs={{0,8},{2,10},{4,12},{6,14},{8,16},{10,18},{12,20},{14,22},{16,24},... | collective-permute-start | bytes 2359304 | tf_op jit(solution)/shard_map/ppermute | solution.py:429
  283.8 20.9 %collective-permute-start.23 = (bf16[192,2048]{1,0:T(8,128)(2,1)S(1)}, bf16[192,2048]{1,0:T(8,128)(2,1)S(1)}, u32[]{:S(2)}, u32[]{:S(2)}) collective-permute-start(bf16[192,2048]{1,0:T(8,128)(2,1)S(1)} %get-tuple-element.17), channel_id=1, source_target_pairs={{8,0},{10,2},{12,4},{14,6},{16,8},{18,10},{20,12},{22,14},{24,16},... | collective-permute-start | bytes 2359304 | tf_op jit(solution)/shard_map/ppermute | solution.py:429
  285.1 20.7 %collective-permute-start.20 = (bf16[192,2048]{1,0:T(8,128)(2,1)S(1)}, bf16[192,2048]{1,0:T(8,128)(2,1)S(1)}, u32[]{:S(2)}, u32[]{:S(2)}) collective-permute-start(bf16[192,2048]{1,0:T(8,128)(2,1)S(1)} %get-tuple-element.18), channel_id=1, source_target_pairs={{0,8},{2,10},{4,12},{6,14},{8,16},{10,18},{12,20},{14,22},{16,24},... | collective-permute-start | bytes 2359304 | tf_op jit(solution)/shard_map/ppermute | solution.py:429
  (25 other events, 376.5 us)
where the time goes:
time: 309 us; the launch traced here: 307 us
  waiting for transfers between devices  138 us (45%)
  starting transfers between devices  64.2 us (21%)
  Pallas kernels  47.3 us (15%)
  local copies, waits for them, and re-layouts  38.8 us (13%)
  other arithmetic  17.1 us (6%)
    ppermute x12, waiting for transfers between devices, along_line(): return lax.ppermute(value, 'sp', pairs)  96.3 us
    ppermute x12, starting transfers between devices, along_line(): return lax.ppermute(value, 'sp', pairs)  53.8 us
    pallas_call x2, Pallas kernels, feed(): pl.pallas_call(hidden_kernel, grid=(rows // block,), out_shape=jax.ShapeD...  23.5 us
    pallas_call x1, Pallas kernels, mix(): pl.pallas_call(functools.partial(mixer_kernel, n, conv_w.shape[0]), out_s...  20.2 us
    ppermute x4, waiting for transfers between devices, round_plane(): return lax.ppermute(value, 'sp', pairs)  19.7 us
    ppermute x3, waiting for transfers between devices, round_line(): return lax.ppermute(value, 'sp', pairs)  19.5 us
    ppermute x4, local copies, waits for them, and re-layouts, round_plane(): return lax.ppermute(value, 'sp', pairs)  13.3 us
    concatenate x2, other arithmetic, feed_forward(): out = feed(jnp.concatenate(tokens, axis=0), pieces)  7.5 us
  transfers between devices with their start and end apart: 24, of which 14 were waited for; matrix products, arithmetic and copies ran while one was open for 15% of the time, Pallas kernels for 8%

commit v1 on v0

--- a/solution.py
+++ b/solution.py
@@ -252,19 +252,20 @@
     line_at = lax.axis_index("sp") // plane
     for z in range(line):
         units = pl.ds(z * part, part)
-        flat = down_ref[units, :].astype(jnp.float32).T.astype(jnp.bfloat16)
+        gate = gate_ref[:, units].astype(jnp.float32).T.astype(jnp.bfloat16)
+        up = up_ref[:, units].astype(jnp.float32).T.astype(jnp.bfloat16)
         for s in range(line):
 
             @pl.when(lax.rem(line_at + s, line) == z)
             def _():
-                out_refs[s][0, 0] = gate_ref[:, units]
-                out_refs[s][1, 0] = up_ref[:, units]
-                out_refs[s][2, 0] = flat
+                out_refs[s][0] = gate
+                out_refs[s][1] = up
+                out_refs[s][2] = down_ref[units, :]
 
 
 def pack(line, plane, w_gate, w_up, w_down):
     rows, units = w_gate.shape
-    shape = jax.ShapeDtypeStruct((3, 1, rows, units // line), w_gate.dtype)
+    shape = jax.ShapeDtypeStruct((3, units // line, rows), w_gate.dtype)
     return pl.pallas_call(
         functools.partial(pack_kernel, line, plane),
         out_shape=[shape] * line,
@@ -343,43 +344,47 @@
     )(own, up_sum, down_sum, stream, out_gain[None, :])
 
 
-def hidden_kernel(tokens_ref, *refs):
-    weights, out_ref = refs[:-1], refs[-1]
-    gate = upward = None
-    at = 0
-    for w in weights:
-        block = tokens_ref[:, at : at + w.shape[1]]
-        g = jnp.dot(block, w[0], preferred_element_type=jnp.float32)
-        u = jnp.dot(block, w[1], preferred_element_type=jnp.float32)
-        gate = g if gate is None else gate + g
-        upward = u if upward is None else upward + u
-        at += w.shape[1]
-    hidden = (jax.nn.silu(gate) * upward).astype(jnp.bfloat16)
-    at = 0
-    for w in weights:
-        out_ref[:, at : at + w.shape[1]] = lax.dot_general(
-            hidden, w[2], (((1,), (1,)), ((), ())), preferred_element_type=jnp.float32
-        ).astype(jnp.bfloat16)
-        at += w.shape[1]
+def feed_kernel(count, *refs):
+    tokens, weights, outs = refs[:count], refs[count:-count], refs[-count:]
+    over_features = (((1,), (1,)), ((), ()))
+    for token_ref, out_ref in zip(tokens, outs):
+        gate = upward = None
+        at = 0
+        for w in weights:
+            size = w.shape[2]
+            block = token_ref[:, at : at + size]
+            g = lax.dot_general(block, w[0], over_features, preferred_element_type=jnp.float32)
+            u = lax.dot_general(block, w[1], over_features, preferred_element_type=jnp.float32)
+            gate = g if gate is None else gate + g
+            upward = u if upward is None else upward + u
+            at += size
+        hidden = (jax.nn.silu(gate) * upward).astype(jnp.bfloat16)
+        at = 0
+        for w in weights:
+            size = w.shape[2]
+            out_ref[:, at : at + size] = jnp.dot(
+                hidden, w[2], preferred_element_type=jnp.float32
+            ).astype(jnp.bfloat16)
+            at += size
 
 
 def feed(tokens, pieces):
-    rows, width = tokens.shape
-    block = rows // 2
-    part = pieces[0].shape[2]
+    rows, width = tokens[0].shape
+    count = len(tokens)
+    part = pieces[0].shape[1]
     return pl.pallas_call(
-        hidden_kernel,
-        grid=(rows // block,),
-        out_shape=jax.ShapeDtypeStruct((rows, width), jnp.bfloat16),
-        in_specs=[pl.BlockSpec((block, width), lambda i: (i, 0))]
-        + [pl.BlockSpec(p.shape, lambda i: (0, 0, 0)) for p in pieces],
-        out_specs=pl.BlockSpec((block, width), lambda i: (i, 0)),
+        functools.partial(feed_kernel, count),
+        out_shape=[jax.ShapeDtypeStruct((rows, width), jnp.bfloat16)] * count,
+        in_specs=[VMEM] * (count + len(pieces)),
+        out_specs=[VMEM] * count,
         compiler_params=pltpu.CompilerParams(vmem_limit_bytes=48 * 1024 * 1024),
         cost_estimate=pl.CostEstimate(
-            flops=6 * rows * width * part, bytes_accessed=6 * width * part, transcendentals=0
+            flops=6 * count * rows * width * part,
+            bytes_accessed=6 * width * part,
+            transcendentals=0,
         ),
         name="feed",
-    )(tokens, *pieces)
+    )(*tokens, *pieces)
 
 
 def rms_scale(values, gains):
@@ -452,23 +457,22 @@
     else:
         packed = jnp.stack(
             [
-                jnp.stack([w[:, z * part : (z + 1) * part] for z in range(line)])
+                jnp.stack([w[:, z * part : (z + 1) * part].T for z in range(line)])
                 for w in (w_gate, w_up)
             ]
-            + [w_down.reshape(line, part, rows).transpose(0, 2, 1)],
+            + [w_down.reshape(line, part, rows)],
             axis=1,
         )
         bundles = [
-            lax.dynamic_index_in_dim(packed, (line_at + s) % line, 0, True).transpose(1, 0, 2, 3)
-            for s in range(line)
+            lax.dynamic_index_in_dim(packed, (line_at + s) % line, 0, False) for s in range(line)
         ]
-    stack = jnp.zeros((3, line, rows, part), w_gate.dtype)
-    stack = lax.dynamic_update_slice_in_dim(stack, bundles[0], line_at, 1)
+    stack = jnp.zeros((3, part, line * rows), w_gate.dtype)
+    stack = lax.dynamic_update_slice_in_dim(stack, bundles[0], line_at * rows, 2)
     arrived = []
     for s in range(1, line):
         arrived.append((s, round_line(bundles[s], s)))
     for s, piece in arrived:
-        stack = lax.dynamic_update_slice_in_dim(stack, piece, (line_at - s) % line, 1)
+        stack = lax.dynamic_update_slice_in_dim(stack, piece, (line_at - s) % line * rows, 2)
     from_ring = {0: [stack]}
     ahead = behind = stack
     for k in range(1, plane // 2):
@@ -476,8 +480,9 @@
         behind = round_plane(behind, 1)
         from_ring[k] = [ahead]
         from_ring[plane - k] = [behind]
-    low = round_plane(ahead[:, : line // 2], -1)
-    high = round_plane(behind[:, line // 2 :], 1)
+    middle = line // 2 * rows
+    low = round_plane(ahead[:, :, :middle], -1)
+    high = round_plane(behind[:, :, middle:], 1)
     from_ring[plane // 2] = [low, high]
     ring_at = jnp.asarray(ring_of)[plane_at]
 
@@ -522,20 +527,19 @@
     pieces = []
     for j in range(plane):
         for piece in from_ring[j]:
-            pieces.append(piece.reshape(3, piece.shape[1] * rows, part))
+            pieces.append(piece)
 
     def feed_forward(chosen):
         own_rows = jnp.concatenate([slots[k] for k in chosen], axis=0)
         tokens = [own_rows] + [shift(own_rows, "tp", -i) for i in range(1, tp)]
-        out = feed(jnp.concatenate(tokens, axis=0), pieces)
-        out = out.reshape(tp, len(chosen) * share, width)
+        out = feed(tokens, pieces)
         total = out[0].astype(jnp.float32)
         for i in range(1, tp):
             total = total + shift(out[i], "tp", i).astype(jnp.float32)
         return {k: total[a * share : (a + 1) * share] for a, k in enumerate(chosen)}
 
     sums = {}
-    for chosen in ([2, 0], [1, 3]) if line == 4 else ([k for k in range(line)],):
+    for chosen in ([1, 3], [2, 0]):
         sums.update(feed_forward(chosen))
 
     up_sum = down_sum = None

time: 309 us -> 294 us (0.951)
  local copies, waits for them, and re-layouts: 38.8 us -> 20.4 us
  waiting for transfers between devices: 138 us -> 151 us
  other arithmetic: 17.1 us -> 8.52 us
    ppermute x4, waiting for transfers between devices: 19.7 us -> 35.5 us  [round_plane(): return lax.ppermute(value, 'sp', pairs)]
    ppermute x4 -> x0, local copies, waits for them, and re-layouts: 13.3 us -> none  [round_plane(): return lax.ppermute(value, 'sp', pairs)]
    concatenate x2 -> x0, other arithmetic: 7.5 us -> none  [feed_forward(): out = feed(jnp.concatenate(tokens, axis=0), pieces)]
    pallas_call x4 -> x0, local copies, waits for them, and re-layouts: 3.46 us -> none  [pack(): pl.pallas_call(functools.partial(pack_kernel, line, plane), out_shape=[sh...]
    slice x4 -> x2, local copies, waits for them, and re-layouts: 7.88 us -> 4.61 us  [the longest x1 2.31 us: shards(): high = round_plane(behind[:, :, middle:], 1)]
    dynamic_update_slice x5 -> x4, local copies, waits for them, and re-layouts: 6.23 us -> 6.65 us  [the longest x3 5.78 us: shards(): lax.dynamic_update_slice_in_dim(stack, piece, (line_at - s) % line * rows...]
  transfers between devices with their start and end apart: 24 -> 24, of which waited for: 14 -> 14; matrix products, arithmetic and copies ran while one was open for 15% -> 7% of each run, Pallas kernels for 8% -> 9%
where the time goes in v1:
time: 294 us; the launch traced here: 293 us
  waiting for transfers between devices  151 us (51%)
  starting transfers between devices  62.6 us (21%)
  Pallas kernels  49.2 us (17%)
  local copies, waits for them, and re-layouts  20.4 us (7%)
  other arithmetic  8.52 us (3%)
    ppermute x12, waiting for transfers between devices, along_line(): return lax.ppermute(value, 'sp', pairs)  96.1 us
    ppermute x12, starting transfers between devices, along_line(): return lax.ppermute(value, 'sp', pairs)  52.1 us
    ppermute x4, waiting for transfers between devices, round_plane(): return lax.ppermute(value, 'sp', pairs)  35.5 us
    pallas_call x2, Pallas kernels, feed(): pl.pallas_call(functools.partial(feed_kernel, count), out_shape=[jax.Shap...  23.9 us
    pallas_call x1, Pallas kernels, mix(): pl.pallas_call(functools.partial(mixer_kernel, n, conv_w.shape[0]), out_s...  20.1 us
    ppermute x3, waiting for transfers between devices, round_line(): return lax.ppermute(value, 'sp', pairs)  16.8 us
  transfers between devices with their start and end apart: 24, of which 14 were waited for; matrix products, arithmetic and copies ran while one was open for 7% of the time, Pallas kernels for 9%

profile of v1, /device:TPU:0, one launch (start us, length us, event | category | flops | bytes accessed | tf_op | source)
XLA Modules:
  0.0 293.4 jit_solution(17907407628988699426)
XLA Ops:
  6.3 20.1 %mixer.1 = bf16[384,1024]{1,0:T(8,128)(2,1)S(1)} custom-call(bf16[384,1024]{1,0:T(8,128)(2,1)S(1)} %copy-done.3, bf16[384,1024]{1,0:T(8,128)(2,1)S(1)} %copy-done.4, f32[4,1024]{1,0:T(4,128)S(1)} %copy-done.10, bf16[8,128,128]{2,1,0:T(8,128)(2,1)S(1)} %get-tuple-element.38.ga_ref, bf16[8,128,128]{2,1,0:T(8,128)(2,1)S(1)} %get-tuple-element.39.gx_ref, ...), custom_call_target="tpu_custom_call" | custom-call | flops 15360000 | bytes 4718592 | tf_op jit(solution)/shard_map/mixer/pallas_call | solution.py:206
  33.1 5.5 %collective-permute-start.1 = (bf16[192,2048]{1,0:T(8,128)(2,1)S(1)}, bf16[192,2048]{1,0:T(8,128)(2,1)}, u32[]{:S(2)}, u32[]{:S(2)}) collective-permute-start(bf16[192,2048]{1,0:T(8,128)(2,1)S(1)} %get-tuple-element.15), channel_id=1, source_target_pairs={{0,8},{2,10},{4,12},{6,14},{8,16},{10,18},{12,20},{14,22},{16,24},... | collective-permute-start | bytes 2359304 | tf_op jit(solution)/shard_map/ppermute | solution.py:434
  38.6 14.8 %collective-permute-done.3 = bf16[192,2048]{1,0:T(8,128)(2,1)} collective-permute-done((bf16[192,2048]{1,0:T(8,128)(2,1)S(1)}, bf16[192,2048]{1,0:T(8,128)(2,1)}, u32[]{:S(2)}, u32[]{:S(2)}) %collective-permute-start.3) | collective-permute-done | bytes 786464 | tf_op jit(solution)/shard_map/ppermute | solution.py:434
  54.7 2.4 pack.1
  57.9 2.6 collective-permute-start.6
  60.5 3.0 %collective-permute-start.7 = (bf16[3,704,128]{2,1,0:T(8,128)(2,1)}, bf16[3,704,128]{2,1,0:T(8,128)(2,1)}, u32[]{:S(2)}, u32[]{:S(2)}) collective-permute-start(bf16[3,704,128]{2,1,0:T(8,128)(2,1)} %get-tuple-element.18), channel_id=1, source_target_pairs={{0,16},{2,18},{4,20},{6,22},{8,24},{10,26},{12,28},{14,30},{16,0},... | collective-permute-start | bytes 1622024 | tf_op jit(solution)/shard_map/ppermute | solution.py:442
  63.5 2.8 collective-permute-start.2
  66.3 22.6 %collective-permute-done.4 = bf16[192,2048]{1,0:T(8,128)(2,1)} collective-permute-done((bf16[192,2048]{1,0:T(8,128)(2,1)}, bf16[192,2048]{1,0:T(8,128)(2,1)}, u32[]{:S(2)}, u32[]{:S(2)}) %collective-permute-start.4) | collective-permute-done | bytes 786464 | tf_op jit(solution)/shard_map/ppermute | solution.py:434
  94.5 16.8 %collective-permute-done.7 = bf16[3,704,128]{2,1,0:T(8,128)(2,1)} collective-permute-done((bf16[3,704,128]{2,1,0:T(8,128)(2,1)}, bf16[3,704,128]{2,1,0:T(8,128)(2,1)}, u32[]{:S(2)}, u32[]{:S(2)}) %collective-permute-start.7) | collective-permute-done | bytes 540704 | tf_op jit(solution)/shard_map/ppermute | solution.py:442
  117.2 13.0 %collective-permute-start.15 = (bf16[192,2048]{1,0:T(8,128)(2,1)}, bf16[192,2048]{1,0:T(8,128)(2,1)}, u32[]{:S(2)}, u32[]{:S(2)}) collective-permute-start(bf16[192,2048]{1,0:T(8,128)(2,1)} %collective-permute-done.2), channel_id=1, source_target_pairs={{0,8},{2,10},{4,12},{6,14},{8,16},{10,18},{12,20},{14,22},{16,24},... | collective-permute-start | bytes 2359304 | tf_op jit(solution)/shard_map/ppermute | solution.py:434
  131.4 11.3 %collective-permute-done.15 = bf16[192,2048]{1,0:T(8,128)(2,1)} collective-permute-done((bf16[192,2048]{1,0:T(8,128)(2,1)}, bf16[192,2048]{1,0:T(8,128)(2,1)}, u32[]{:S(2)}, u32[]{:S(2)}) %collective-permute-start.15) | collective-permute-done | bytes 786464 | tf_op jit(solution)/shard_map/ppermute | solution.py:434
  145.3 15.8 %collective-permute-done.11.refs_6_ = bf16[3,704,512]{2,1,0:T(8,128)(2,1)} collective-permute-done((bf16[3,704,512]{2,1,0:T(8,128)(2,1)}, bf16[3,704,512]{2,1,0:T(8,128)(2,1)}, u32[]{:S(2)}, u32[]{:S(2)}) %collective-permute-start.11) | collective-permute-done | bytes 2162720 | tf_op jit(solution)/shard_map/ppermute | solution.py:450
  161.1 2.3 slice.45
  165.0 2.3 slice.44
  169.3 16.2 %collective-permute-done.12.refs_5_ = bf16[3,704,256]{2,1,0:T(8,128)(2,1)} collective-permute-done((bf16[3,704,256]{2,1,0:T(8,128)(2,1)}, bf16[3,704,256]{2,1,0:T(8,128)(2,1)}, u32[]{:S(2)}, u32[]{:S(2)}) %collective-permute-start.12) | collective-permute-done | bytes 1081376 | tf_op jit(solution)/shard_map/ppermute | solution.py:450
  185.4 3.6 %collective-permute-done.10.refs_4_ = bf16[3,704,256]{2,1,0:T(8,128)(2,1)} collective-permute-done((bf16[3,704,256]{2,1,0:T(8,128)(2,1)}, bf16[3,704,256]{2,1,0:T(8,128)(2,1)}, u32[]{:S(2)}, u32[]{:S(2)}) %collective-permute-start.10) | collective-permute-done | bytes 1081376 | tf_op jit(solution)/shard_map/ppermute | solution.py:450
  189.0 12.0 %feed.3 = (bf16[384,2048]{1,0:T(8,128)(2,1)S(1)}, bf16[384,2048]{1,0:T(8,128)(2,1)S(1)}) custom-call(bf16[384,2048]{1,0:T(8,128)(2,1)} %pad_maximum_fusion.1.refs_0_, bf16[384,2048]{1,0:T(8,128)(2,1)} %collective-permute-done.16.refs_1_, bf16[3,704,512]{2,1,0:T(8,128)(2,1)} %constant_dynamic-update-slice_fusion.refs_2_, ...), custom_call_target="tpu_custom_call" | custom-call | flops 6643777536 | bytes 8650752 | tf_op jit(solution)/shard_map/feed/pallas_call | solution.py:375
  202.3 12.0 %feed.2 = (bf16[384,2048]{1,0:T(8,128)(2,1)S(1)}, bf16[384,2048]{1,0:T(8,128)(2,1)S(1)}) custom-call(bf16[384,2048]{1,0:T(8,128)(2,1)} %copy-done.15, bf16[384,2048]{1,0:T(8,128)(2,1)} %copy-done.17, bf16[3,704,512]{2,1,0:T(8,128)(2,1)} %constant_dynamic-update-slice_fusion.refs_2_, bf16[3,704,512]{2,1,0:T(8,128)(2,1)} %collective-permute-done.9.refs_3_, ...), custom_call_target="tpu_custom_call" | custom-call | flops 6643777536 | bytes 8650752 | tf_op jit(solution)/shard_map/feed/pallas_call | solution.py:375
  216.9 13.0 %collective-permute-start.18 = (bf16[192,2048]{1,0:T(8,128)(2,1)S(1)}, bf16[192,2048]{1,0:T(8,128)(2,1)S(1)}, u32[]{:S(2)}, u32[]{:S(2)}) collective-permute-start(bf16[192,2048]{1,0:T(8,128)(2,1)S(1)} %get-tuple-element.31), channel_id=1, source_target_pairs={{0,8},{2,10},{4,12},{6,14},{8,16},{10,18},{12,20},{14,22},{16,24},... | collective-permute-start | bytes 2359304 | tf_op jit(solution)/shard_map/ppermute | solution.py:434
  230.5 14.9 %collective-permute-done.21 = bf16[192,2048]{1,0:T(8,128)(2,1)S(1)} collective-permute-done((bf16[192,2048]{1,0:T(8,128)(2,1)S(1)}, bf16[192,2048]{1,0:T(8,128)(2,1)S(1)}, u32[]{:S(2)}, u32[]{:S(2)}) %collective-permute-start.21) | collective-permute-done | bytes 786464 | tf_op jit(solution)/shard_map/ppermute | solution.py:434
  248.5 5.1 %collective-permute-start.19 = (bf16[192,2048]{1,0:T(8,128)(2,1)S(1)}, bf16[192,2048]{1,0:T(8,128)(2,1)S(1)}, u32[]{:S(2)}, u32[]{:S(2)}) collective-permute-start(bf16[192,2048]{1,0:T(8,128)(2,1)S(1)} %get-tuple-element.28), channel_id=1, source_target_pairs={{0,8},{2,10},{4,12},{6,14},{8,16},{10,18},{12,20},{14,22},{16,24},... | collective-permute-start | bytes 2359304 | tf_op jit(solution)/shard_map/ppermute | solution.py:434
  253.6 14.9 %collective-permute-done.22 = bf16[192,2048]{1,0:T(8,128)(2,1)S(1)} collective-permute-done((bf16[192,2048]{1,0:T(8,128)(2,1)S(1)}, bf16[192,2048]{1,0:T(8,128)(2,1)S(1)}, u32[]{:S(2)}, u32[]{:S(2)}) %collective-permute-start.22) | collective-permute-done | bytes 786464 | tf_op jit(solution)/shard_map/ppermute | solution.py:434
  271.5 5.1 %collective-permute-start.20 = (bf16[192,2048]{1,0:T(8,128)(2,1)S(1)}, bf16[192,2048]{1,0:T(8,128)(2,1)S(1)}, u32[]{:S(2)}, u32[]{:S(2)}) collective-permute-start(bf16[192,2048]{1,0:T(8,128)(2,1)S(1)} %get-tuple-element.26), channel_id=1, source_target_pairs={{0,8},{2,10},{4,12},{6,14},{8,16},{10,18},{12,20},{14,22},{16,24},... | collective-permute-start | bytes 2359304 | tf_op jit(solution)/shard_map/ppermute | solution.py:434
  276.5 14.0 %collective-permute-done.23.down_ref = bf16[192,2048]{1,0:T(8,128)(2,1)S(1)} collective-permute-done((bf16[192,2048]{1,0:T(8,128)(2,1)S(1)}, bf16[192,2048]{1,0:T(8,128)(2,1)S(1)}, u32[]{:S(2)}, u32[]{:S(2)}) %collective-permute-start.23) | collective-permute-done | bytes 786464 | tf_op jit(solution)/shard_map/ppermute | solution.py:434
  (89 shorter events, 47.1 us)
Async XLA Ops:
  28.4 2.4 collective-permute-start
  31.8 21.6 %collective-permute-start.3 = (bf16[192,2048]{1,0:T(8,128)(2,1)S(1)}, bf16[192,2048]{1,0:T(8,128)(2,1)}, u32[]{:S(2)}, u32[]{:S(2)}) collective-permute-start(bf16[192,2048]{1,0:T(8,128)(2,1)S(1)} %get-tuple-element.15), channel_id=1, source_target_pairs={{8,0},{10,2},{12,4},{14,6},{16,8},{18,10},{20,12},{22,14},{24,16},... | collective-permute-start | bytes 2359304 | tf_op jit(solution)/shard_map/ppermute | solution.py:434
  33.1 30.3 %collective-permute-start.1 = (bf16[192,2048]{1,0:T(8,128)(2,1)S(1)}, bf16[192,2048]{1,0:T(8,128)(2,1)}, u32[]{:S(2)}, u32[]{:S(2)}) collective-permute-start(bf16[192,2048]{1,0:T(8,128)(2,1)S(1)} %get-tuple-element.15), channel_id=1, source_target_pairs={{0,8},{2,10},{4,12},{6,14},{8,16},{10,18},{12,20},{14,22},{16,24},... | collective-permute-start | bytes 2359304 | tf_op jit(solution)/shard_map/ppermute | solution.py:434
  53.4 35.4 %collective-permute-start.4 = (bf16[192,2048]{1,0:T(8,128)(2,1)}, bf16[192,2048]{1,0:T(8,128)(2,1)}, u32[]{:S(2)}, u32[]{:S(2)}) collective-permute-start(bf16[192,2048]{1,0:T(8,128)(2,1)} %collective-permute-done.3), channel_id=1, source_target_pairs={{8,0},{10,2},{12,4},{14,6},{16,8},{18,10},{20,12},{22,14},{24,16},... | collective-permute-start | bytes 2359304 | tf_op jit(solution)/shard_map/ppermute | solution.py:434
  57.9 34.7 %collective-permute-start.6 = (bf16[3,704,128]{2,1,0:T(8,128)(2,1)}, bf16[3,704,128]{2,1,0:T(8,128)(2,1)}, u32[]{:S(2)}, u32[]{:S(2)}) collective-permute-start(bf16[3,704,128]{2,1,0:T(8,128)(2,1)} %get-tuple-element.17), channel_id=1, source_target_pairs={{0,8},{2,10},{4,12},{6,14},{8,16},{10,18},{12,20},{14,22},{16,24},... | collective-permute-start | bytes 1622024 | tf_op jit(solution)/shard_map/ppermute | solution.py:442
  60.5 50.7 %collective-permute-start.7 = (bf16[3,704,128]{2,1,0:T(8,128)(2,1)}, bf16[3,704,128]{2,1,0:T(8,128)(2,1)}, u32[]{:S(2)}, u32[]{:S(2)}) collective-permute-start(bf16[3,704,128]{2,1,0:T(8,128)(2,1)} %get-tuple-element.18), channel_id=1, source_target_pairs={{0,16},{2,18},{4,20},{6,22},{8,24},{10,26},{12,28},{14,30},{16,0},... | collective-permute-start | bytes 1622024 | tf_op jit(solution)/shard_map/ppermute | solution.py:442
  63.5 53.7 %collective-permute-start.2 = (bf16[192,2048]{1,0:T(8,128)(2,1)}, bf16[192,2048]{1,0:T(8,128)(2,1)}, u32[]{:S(2)}, u32[]{:S(2)}) collective-permute-start(bf16[192,2048]{1,0:T(8,128)(2,1)} %collective-permute-done.1), channel_id=1, source_target_pairs={{0,8},{2,10},{4,12},{6,14},{8,16},{10,18},{12,20},{14,22},{16,24},... | collective-permute-start | bytes 2359304 | tf_op jit(solution)/shard_map/ppermute | solution.py:434
  66.3 46.9 %collective-permute-start.8 = (bf16[3,704,128]{2,1,0:T(8,128)(2,1)}, bf16[3,704,128]{2,1,0:T(8,128)(2,1)}, u32[]{:S(2)}, u32[]{:S(2)}) collective-permute-start(bf16[3,704,128]{2,1,0:T(8,128)(2,1)} %get-tuple-element.19), channel_id=1, source_target_pairs={{0,24},{2,26},{4,28},{6,30},{8,0},{10,2},{12,4},{14,6},{16,8},{18,... | collective-permute-start | bytes 1622024 | tf_op jit(solution)/shard_map/ppermute | solution.py:442
  88.9 41.3 %collective-permute-start.14 = (bf16[192,2048]{1,0:T(8,128)(2,1)}, bf16[192,2048]{1,0:T(8,128)(2,1)}, u32[]{:S(2)}, u32[]{:S(2)}) collective-permute-start(bf16[192,2048]{1,0:T(8,128)(2,1)} %collective-permute-done.4), channel_id=1, source_target_pairs={{8,0},{10,2},{12,4},{14,6},{16,8},{18,10},{20,12},{22,14},{24,16},... | collective-permute-start | bytes 2359304 | tf_op jit(solution)/shard_map/ppermute | solution.py:434
  115.1 46.0 %collective-permute-start.11 = (bf16[3,704,512]{2,1,0:T(8,128)(2,1)}, bf16[3,704,512]{2,1,0:T(8,128)(2,1)}, u32[]{:S(2)}, u32[]{:S(2)}) collective-permute-start(bf16[3,704,512]{2,1,0:T(8,128)(2,1)} %constant_dynamic-update-slice_fusion.refs_2_), channel_id=1, source_target_pairs={{0,2},{2,6},{6,4},{4,0},{8,10},{10,14},{14,12},{12,8},{16,18},{18,... | collective-permute-start | bytes 6488072 | tf_op jit(solution)/shard_map/ppermute | solution.py:450
  116.7 48.3 %collective-permute-start.9 = (bf16[3,704,512]{2,1,0:T(8,128)(2,1)}, bf16[3,704,512]{2,1,0:T(8,128)(2,1)}, u32[]{:S(2)}, u32[]{:S(2)}) collective-permute-start(bf16[3,704,512]{2,1,0:T(8,128)(2,1)} %constant_dynamic-update-slice_fusion.refs_2_), channel_id=1, source_target_pairs={{0,4},{2,0},{6,2},{4,6},{8,12},{10,8},{14,10},{12,14},{16,20},{18,... | collective-permute-start | bytes 6488072 | tf_op jit(solution)/shard_map/ppermute | solution.py:450
  117.2 25.6 %collective-permute-start.15 = (bf16[192,2048]{1,0:T(8,128)(2,1)}, bf16[192,2048]{1,0:T(8,128)(2,1)}, u32[]{:S(2)}, u32[]{:S(2)}) collective-permute-start(bf16[192,2048]{1,0:T(8,128)(2,1)} %collective-permute-done.2), channel_id=1, source_target_pairs={{0,8},{2,10},{4,12},{6,14},{8,16},{10,18},{12,20},{14,22},{16,24},... | collective-permute-start | bytes 2359304 | tf_op jit(solution)/shard_map/ppermute | solution.py:434
  145.3 43.7 %collective-permute-start.16 = (bf16[384,2048]{1,0:T(8,128)(2,1)}, bf16[384,2048]{1,0:T(8,128)(2,1)}, u32[]{:S(2)}, u32[]{:S(2)}) collective-permute-start(bf16[384,2048]{1,0:T(8,128)(2,1)} %pad_maximum_fusion.1.refs_0_), channel_id=1, source_target_pairs={{0,1},{1,0},{2,3},{3,2},{4,5},{5,4},{6,7},{7,6},{8,9},{9,8},{10,11... | collective-permute-start | bytes 4718600 | tf_op jit(solution)/shard_map/ppermute | solution.py:396
  163.4 22.0 %collective-permute-start.12 = (bf16[3,704,256]{2,1,0:T(8,128)(2,1)}, bf16[3,704,256]{2,1,0:T(8,128)(2,1)}, u32[]{:S(2)}, u32[]{:S(2)}) collective-permute-start(bf16[3,704,256]{2,1,0:T(8,128)(2,1)} %slice.45), channel_id=1, source_target_pairs={{0,2},{2,6},{6,4},{4,0},{8,10},{10,14},{14,12},{12,8},{16,18},{18,... | collective-permute-start | bytes 3244040 | tf_op jit(solution)/shard_map/ppermute | solution.py:450
  167.3 21.7 %collective-permute-start.10 = (bf16[3,704,256]{2,1,0:T(8,128)(2,1)}, bf16[3,704,256]{2,1,0:T(8,128)(2,1)}, u32[]{:S(2)}, u32[]{:S(2)}) collective-permute-start(bf16[3,704,256]{2,1,0:T(8,128)(2,1)} %slice.44), channel_id=1, source_target_pairs={{0,4},{2,0},{6,2},{4,6},{8,12},{10,8},{14,10},{12,14},{16,20},{18,... | collective-permute-start | bytes 3244040 | tf_op jit(solution)/shard_map/ppermute | solution.py:450
  169.2 31.9 %collective-permute-start.5 = (bf16[384,2048]{1,0:T(8,128)(2,1)S(1)}, bf16[384,2048]{1,0:T(8,128)(2,1)S(1)}, u32[]{:S(2)}, u32[]{:S(2)}) collective-permute-start(bf16[384,2048]{1,0:T(8,128)(2,1)S(1)} %pad_maximum_fusion.refs_0_), channel_id=1, source_target_pairs={{0,1},{1,0},{2,3},{3,2},{4,5},{5,4},{6,7},{7,6},{8,9},{9,8},{10,11... | collective-permute-start | bytes 4718600 | tf_op jit(solution)/shard_map/ppermute | solution.py:396
  200.9 13.9 %collective-permute-start.17 = (bf16[384,2048]{1,0:T(8,128)(2,1)S(1)}, bf16[384,2048]{1,0:T(8,128)(2,1)S(1)}, u32[]{:S(2)}, u32[]{:S(2)}) collective-permute-start(bf16[384,2048]{1,0:T(8,128)(2,1)S(1)} %get-tuple-element.23), channel_id=1, source_target_pairs={{0,1},{1,0},{2,3},{3,2},{4,5},{5,4},{6,7},{7,6},{8,9},{9,8},{10,11... | collective-permute-start | bytes 4718600 | tf_op jit(solution)/shard_map/ppermute | solution.py:396
  214.2 15.7 %collective-permute-start.13 = (bf16[384,2048]{1,0:T(8,128)(2,1)S(1)}, bf16[384,2048]{1,0:T(8,128)(2,1)S(1)}, u32[]{:S(2)}, u32[]{:S(2)}) collective-permute-start(bf16[384,2048]{1,0:T(8,128)(2,1)S(1)} %get-tuple-element.21), channel_id=1, source_target_pairs={{0,1},{1,0},{2,3},{3,2},{4,5},{5,4},{6,7},{7,6},{8,9},{9,8},{10,11... | collective-permute-start | bytes 4718600 | tf_op jit(solution)/shard_map/ppermute | solution.py:396
  215.6 29.8 %collective-permute-start.21 = (bf16[192,2048]{1,0:T(8,128)(2,1)S(1)}, bf16[192,2048]{1,0:T(8,128)(2,1)S(1)}, u32[]{:S(2)}, u32[]{:S(2)}) collective-permute-start(bf16[192,2048]{1,0:T(8,128)(2,1)S(1)} %get-tuple-element.30), channel_id=1, source_target_pairs={{8,0},{10,2},{12,4},{14,6},{16,8},{18,10},{20,12},{22,14},{24,16},... | collective-permute-start | bytes 2359304 | tf_op jit(solution)/shard_map/ppermute | solution.py:434
  216.9 29.7 %collective-permute-start.18 = (bf16[192,2048]{1,0:T(8,128)(2,1)S(1)}, bf16[192,2048]{1,0:T(8,128)(2,1)S(1)}, u32[]{:S(2)}, u32[]{:S(2)}) collective-permute-start(bf16[192,2048]{1,0:T(8,128)(2,1)S(1)} %get-tuple-element.31), channel_id=1, source_target_pairs={{0,8},{2,10},{4,12},{6,14},{8,16},{10,18},{12,20},{14,22},{16,24},... | collective-permute-start | bytes 2359304 | tf_op jit(solution)/shard_map/ppermute | solution.py:434
  247.2 21.3 %collective-permute-start.22 = (bf16[192,2048]{1,0:T(8,128)(2,1)S(1)}, bf16[192,2048]{1,0:T(8,128)(2,1)S(1)}, u32[]{:S(2)}, u32[]{:S(2)}) collective-permute-start(bf16[192,2048]{1,0:T(8,128)(2,1)S(1)} %get-tuple-element.27), channel_id=1, source_target_pairs={{8,0},{10,2},{12,4},{14,6},{16,8},{18,10},{20,12},{22,14},{24,16},... | collective-permute-start | bytes 2359304 | tf_op jit(solution)/shard_map/ppermute | solution.py:434
  248.5 21.1 %collective-permute-start.19 = (bf16[192,2048]{1,0:T(8,128)(2,1)S(1)}, bf16[192,2048]{1,0:T(8,128)(2,1)S(1)}, u32[]{:S(2)}, u32[]{:S(2)}) collective-permute-start(bf16[192,2048]{1,0:T(8,128)(2,1)S(1)} %get-tuple-element.28), channel_id=1, source_target_pairs={{0,8},{2,10},{4,12},{6,14},{8,16},{10,18},{12,20},{14,22},{16,24},... | collective-permute-start | bytes 2359304 | tf_op jit(solution)/shard_map/ppermute | solution.py:434
  270.2 20.4 %collective-permute-start.23 = (bf16[192,2048]{1,0:T(8,128)(2,1)S(1)}, bf16[192,2048]{1,0:T(8,128)(2,1)S(1)}, u32[]{:S(2)}, u32[]{:S(2)}) collective-permute-start(bf16[192,2048]{1,0:T(8,128)(2,1)S(1)} %get-tuple-element.25), channel_id=1, source_target_pairs={{8,0},{10,2},{12,4},{14,6},{16,8},{18,10},{20,12},{22,14},{24,16},... | collective-permute-start | bytes 2359304 | tf_op jit(solution)/shard_map/ppermute | solution.py:434
  271.5 20.3 %collective-permute-start.20 = (bf16[192,2048]{1,0:T(8,128)(2,1)S(1)}, bf16[192,2048]{1,0:T(8,128)(2,1)S(1)}, u32[]{:S(2)}, u32[]{:S(2)}) collective-permute-start(bf16[192,2048]{1,0:T(8,128)(2,1)S(1)} %get-tuple-element.26), channel_id=1, source_target_pairs={{0,8},{2,10},{4,12},{6,14},{8,16},{10,18},{12,20},{14,22},{16,24},... | collective-permute-start | bytes 2359304 | tf_op jit(solution)/shard_map/ppermute | solution.py:434
  (18 other events, 258.7 us)
